TPU v7x, 32 devices: a whole 2x2x4 slice. The times are simulated.
32 devices in a mesh: ep: 4 (over y, x), tp: 8 (over z, core).
Axes of the slice: x: 2, y: 2, z: 4, core: 2. Of those that a mesh axis runs over, the one named last changes fastest.
Arguments:
- tokens: bfloat16 [2048, 2048], P('ep', 'tp'), may hold values from -6 to 6
- norm_gain: float32 [2048], replicated, may hold values from 0.1 to 1.9
- norm_shift: float32 [2048], replicated, may hold values from -3 to 3
- expert_ids: int32 [2048, 6], P('ep'), may hold values from 0 to 31, all different within a row; in each aligned block of 64 rows (0 to 63, 64 to 127, ...) at most 24 rows name the same one
- affinity: float32 [2048, 6], P('ep'), may hold values from 0.05 to 1
- expert_gate: bfloat16 [32, 2048, 512], P(('ep', 'tp')), may hold values from -0.125 to 0.125
- expert_up: bfloat16 [32, 2048, 512], P(('ep', 'tp')), may hold values from -0.125 to 0.125
- expert_down: bfloat16 [32, 512, 2048], P(('ep', 'tp')), may hold values from -0.25 to 0.25
- shared_gate: bfloat16 [512, 2048], P('tp'), may hold values from -0.125 to 0.125
- shared_up: bfloat16 [512, 2048], P('tp'), may hold values from -0.125 to 0.125
- shared_down: bfloat16 [512, 2048], replicated, may hold values from -0.25 to 0.25
Outputs:
- mixed: bfloat16 [2048, 2048], P(('ep', 'tp'))
Inputs may be any that keep to these rules, and one draw needn't show every extreme that they name: `expert_ids`: each row names 6 different experts; in each aligned block of 64 rows (the rows of one device of tp) no expert is named more than 24 times, and in some blocks an expert is named exactly 24 times.
All inputs are finite; a program needn't handle non-finite values.
Results may differ from a plain program's by a relative error of at most 0.0069.
Values may be sent and summed in bfloat16 or wider, within the bound.
A program may use at most 64 MiB of HBM per device.

v0:
```python
import jax
import jax.numpy as jnp
from jax import lax
from jax.sharding import PartitionSpec as P

ROUTED_SCALE = 2.5
EPSILON = 1e-05


def pair_ranks(flat_ids, expert_count):
    onehot = flat_ids[..., None] == jnp.arange(expert_count, dtype=jnp.int32)
    running = jnp.cumsum(onehot.astype(jnp.int32), axis=-2)
    return jnp.sum(jnp.where(onehot, running, 0), axis=-1) - 1


def expert_rows(tok_rows, w_gate, w_up, w_down):
    gate_act = jnp.dot(tok_rows, w_gate, preferred_element_type=jnp.float32)
    up_act = jnp.dot(tok_rows, w_up, preferred_element_type=jnp.float32)
    hidden = (jax.nn.silu(gate_act) * up_act).astype(jnp.bfloat16)
    return jnp.dot(hidden, w_down, preferred_element_type=jnp.float32).astype(jnp.bfloat16)


def weighted_sum(source_rows, slot_index, pair_weight, top_count):
    total = jnp.zeros((slot_index.shape[0], source_rows.shape[1]), jnp.float32)
    for column in range(top_count):
        picked = jnp.take(source_rows, slot_index[:, column], axis=0, mode="fill", fill_value=0)
        total = total + pair_weight[:, column : column + 1] * picked.astype(jnp.float32)
    return total


def on_device(
    tokens,
    norm_gain,
    norm_shift,
    expert_ids,
    affinity,
    expert_gate,
    expert_up,
    expert_down,
    shared_gate,
    shared_up,
    shared_down,
):
    ep_count = lax.axis_size("ep")
    tp_count = lax.axis_size("tp")
    tp_index = lax.axis_index("tp")
    whole = lax.all_gather(tokens, "tp", axis=1, tiled=True)
    tok_count = whole.shape[0]
    width = whole.shape[1]
    top_count = expert_ids.shape[1]
    block_rows = tok_count // tp_count
    expert_count = ep_count * tp_count
    slot_cap = max(1, 2 * block_rows * top_count // expert_count)
    slot_total = expert_count * slot_cap
    values = whole.astype(jnp.float32)
    center = values - jnp.mean(values, axis=1, keepdims=True)
    spread = jnp.mean(center * center, axis=1, keepdims=True)
    normed = (center * lax.rsqrt(spread + EPSILON) * norm_gain + norm_shift).astype(jnp.bfloat16)
    weights = affinity / jnp.sum(affinity, axis=1, keepdims=True) * ROUTED_SCALE
    contract = (((1,), (1,)), ((), ()))
    shared_g = lax.dot_general(shared_gate, normed, contract, preferred_element_type=jnp.float32)
    shared_u = lax.dot_general(shared_up, normed, contract, preferred_element_type=jnp.float32)
    shared_hidden = (jax.nn.silu(shared_g) * shared_u).astype(jnp.bfloat16)
    own_hidden = lax.all_to_all(shared_hidden, "tp", split_axis=1, concat_axis=0, tiled=True)
    shared_out = lax.dot_general(
        own_hidden, shared_down, (((0,), (0,)), ((), ())), preferred_element_type=jnp.float32
    )
    block_ids = expert_ids.reshape(tp_count, block_rows * top_count)
    ranks = pair_ranks(block_ids, expert_count)
    group_index = block_ids // tp_count
    mine = block_ids % tp_count == tp_index
    block_index = jnp.arange(tp_count, dtype=jnp.int32)[:, None]
    dest = jnp.where(mine, (group_index * tp_count + block_index) * slot_cap + ranks, slot_total)
    token_index = (
        block_index * block_rows
        + jnp.arange(block_rows * top_count, dtype=jnp.int32)[None, :] // top_count
    )
    source_row = (
        jnp.full((slot_total + 1,), tok_count, jnp.int32)
        .at[dest.reshape(-1)]
        .set(token_index.reshape(-1))[:slot_total]
    )
    outgoing = jnp.take(normed, source_row, axis=0, mode="fill", fill_value=0).reshape(
        ep_count, tp_count, slot_cap, width
    )
    incoming = lax.all_to_all(outgoing, "ep", split_axis=0, concat_axis=0, tiled=True)
    result = expert_rows(incoming.reshape(-1, width), expert_gate[0], expert_up[0], expert_down[0])
    returned = lax.all_to_all(
        result.reshape(incoming.shape), "ep", split_axis=0, concat_axis=0, tiled=True
    )
    pair_slot = dest.reshape(tok_count, top_count)
    back_rows = returned.reshape(slot_total, width)
    routed = lax.psum_scatter(
        weighted_sum(back_rows, pair_slot, weights, top_count),
        "tp",
        scatter_dimension=0,
        tiled=True,
    )
    return (routed + shared_out).astype(jnp.bfloat16)


def solution(mesh):
    placed = (
        P("ep", "tp"),
        P(),
        P(),
        P("ep", None),
        P("ep", None),
        P(("ep", "tp"), None, None),
        P(("ep", "tp"), None, None),
        P(("ep", "tp"), None, None),
        P("tp", None),
        P("tp", None),
        P(),
    )
    return jax.shard_map(
        on_device, mesh=mesh, in_specs=placed, out_specs=P(("ep", "tp"), None), check_vma=False
    )
```

profile of v0, /device:TPU:0, one launch (start us, length us, event | category | flops | bytes accessed | tf_op | source)
XLA Modules:
  0.0 271.8 jit_solution(16597467197731617035)
XLA Ops:
  6.5 0.7 all-gather.2.cloned.1.call-update
  7.3 0.9 copy.34
  8.1 0.2 eq.48
  8.3 0.2 reshape.242
  8.5 0.2 eq.52
  8.8 6.9 %reduce-window.6 = s32[8,32,3,128]{3,1,2,0:T(8,128)S(1)} reduce-window(s32[8,32,3,128]{3,1,2,0:T(8,128)S(1)} %fusion.20, s32[]{:T(128)} %constant.82.clone.1), window={size=1x1x1x128 pad=0_0x0_0x0_0x127_0}, to_apply=%region_1.0 | reduce-window | flops 12484608 | bytes 786436 | tf_op jit(solution)/shard_map/reduce-window
  15.8 0.2 slice.78
  15.9 0.2 copy.40
  16.1 0.1 fusion.29
  16.3 0.2 fusion.19
  16.5 0.1 compare_select_fusion
  16.6 11.8 %scatter_custom_fusion = s32[769]{0:T(1024)S(1)} fusion(s32[3072]{0:T(1024)S(1)} %bitcast.82, s32[3072]{0:T(1024)S(1)} %reshape.307, s32[]{:T(128)} %constant.81.clone.1), kind=kCustom, calls=%fused_computation.94 | custom fusion | bytes 3080 | tf_op jit(solution)/shard_map/scatter | solution.py:81
  28.4 0.1 slice.51
  28.5 13.8 %all-gather.2.cloned.1.call-done = bf16[512,2048]{1,0:T(8,128)(2,1)} async-done(((bf16[512,256]{1,0:T(8,128)(2,1)}), bf16[512,2048]{1,0:T(8,128)(2,1)}) %all-gather.2.cloned.1.call-update) | async-done | bytes 2097168 | tf_op jit(solution)/shard_map/all_gather | solution.py:47
  42.3 2.1 convert_reduce_fusion
  44.4 0.1 copy-done.2
  44.5 0.7 fusion.2
  45.2 2.2 fusion.5
  47.4 9.0 %gather_fusion = bf16[768,2048]{1,0:T(8,128)(2,1)} fusion(bf16[512,2048]{1,0:T(8,128)(2,1)} %fusion.5, s32[1024]{0:T(1024)S(1)} %pad_clamp_fusion.6), kind=kCustom, calls=%fused_computation.6 | custom fusion | bytes 6294528 | tf_op jit(solution)/shard_map/jit(_take)/gather | solution.py:83
  56.4 3.9 %broadcast_select_fusion = bf16[4,8,24,2048]{3,2,1,0:T(8,128)(2,1)} fusion(bf16[4,8,24,2048]{3,2,1,0:T(8,128)(2,1)} %bitcast.77, pred[4,8,24]{2,1,0:T(8,128)(4,1)S(1)} %compare_and_fusion), kind=kLoop, calls=%fused_computation.18 | loop fusion | flops 1572864 | bytes 6292224 | tf_op jit(solution)/shard_map/jit(_take)/select_n | solution.py:83
  60.3 4.9 %all-to-all-start = ((bf16[4,8,24,2048]{3,2,1,0:T(8,128)(2,1)}), bf16[4,8,24,2048]{3,2,1,0:T(8,128)(2,1)}, u32[]{:S(2)}, u32[]{:S(2)}) async-start(bf16[4,8,24,2048]{3,2,1,0:T(8,128)(2,1)} %broadcast_select_fusion), calls=%async_computation | async-start | bytes 6291456 | tf_op jit(solution)/shard_map/all_to_all | solution.py:86
  65.2 0.1 add.204
  65.3 0.2 sub.37
  65.5 0.3 fusion.26
  65.8 0.8 slice_reduce_fusion.5
  66.7 35.2 %all-to-all-done = bf16[4,8,24,2048]{3,2,1,0:T(8,128)(2,1)} async-done(((bf16[4,8,24,2048]{3,2,1,0:T(8,128)(2,1)}), bf16[4,8,24,2048]{3,2,1,0:T(8,128)(2,1)}, u32[]{:S(2)}, u32[]{:S(2)}) %all-to-all-start) | async-done | bytes 3145760 | tf_op jit(solution)/shard_map/all_to_all | solution.py:86
  101.9 5.6 %fusion.10 = f32[768,512]{1,0:T(8,128)} fusion(bf16[768,2048]{1,0:T(8,128)(2,1)} %bitcast.5, bf16[1,2048,512]{2,1,0:T(8,128)(2,1)} %param.18), kind=kOutput, calls=%fused_computation.24 | convolution fusion | flops 1610612736 | bytes 6815744 | tf_op jit(solution)/shard_map/dot_general | solution.py:17
  107.4 8.2 %convolution_convert_fusion = bf16[768,2048]{1,0:T(8,128)(2,1)} fusion(bf16[1,512,2048]{2,1,0:T(8,128)(2,1)S(1)} %copy-done, f32[768,512]{1,0:T(8,128)} %fusion.10, bf16[768,2048]{1,0:T(8,128)(2,1)} %bitcast.5, bf16[1,2048,512]{2,1,0:T(8,128)(2,1)} %param.19), kind=kOutput, calls=%fused_computation.17 | convolution fusion | flops 3225157632 | bytes 12058624 | tf_op jit(solution)/shard_map/dot_general | solution.py:20
  115.6 4.6 %all-to-all-start.1 = ((bf16[4,8,24,2048]{3,2,1,0:T(8,128)(2,1)}), bf16[4,8,24,2048]{3,2,1,0:T(8,128)(2,1)}, u32[]{:S(2)}, u32[]{:S(2)}) async-start(bf16[4,8,24,2048]{3,2,1,0:T(8,128)(2,1)} %bitcast.78), calls=%async_computation.1 | async-start | bytes 6291456 | tf_op jit(solution)/shard_map/all_to_all | solution.py:88
  120.5 35.7 %all-to-all-done.1 = bf16[4,8,24,2048]{3,2,1,0:T(8,128)(2,1)} async-done(((bf16[4,8,24,2048]{3,2,1,0:T(8,128)(2,1)}), bf16[4,8,24,2048]{3,2,1,0:T(8,128)(2,1)}, u32[]{:S(2)}, u32[]{:S(2)}) %all-to-all-start.1) | async-done | bytes 3145760 | tf_op jit(solution)/shard_map/all_to_all | solution.py:88
  156.2 7.8 %gather_fusion.6 = bf16[512,2048]{1,0:T(8,128)(2,1)} fusion(bf16[768,2048]{1,0:T(8,128)(2,1)} %bitcast.10, s32[1024]{0:T(1024)S(1)} %pad_clamp_fusion), kind=kCustom, calls=%fused_computation.5.clone | custom fusion | bytes 4196352 | tf_op jit(solution)/shard_map/jit(_take)/gather | solution.py:26
  164.0 7.5 %gather_fusion.5 = bf16[512,2048]{1,0:T(8,128)(2,1)} fusion(bf16[768,2048]{1,0:T(8,128)(2,1)} %bitcast.10, s32[1024]{0:T(1024)S(1)} %pad_clamp_fusion.1), kind=kCustom, calls=%fused_computation.4.clone | custom fusion | bytes 4196352 | tf_op jit(solution)/shard_map/jit(_take)/gather | solution.py:26
  171.6 7.5 %gather_fusion.4 = bf16[512,2048]{1,0:T(8,128)(2,1)} fusion(bf16[768,2048]{1,0:T(8,128)(2,1)} %bitcast.10, s32[1024]{0:T(1024)S(1)} %pad_clamp_fusion.2), kind=kCustom, calls=%fused_computation.3.clone | custom fusion | bytes 4196352 | tf_op jit(solution)/shard_map/jit(_take)/gather | solution.py:26
  179.1 7.5 %gather_fusion.3 = bf16[512,2048]{1,0:T(8,128)(2,1)} fusion(bf16[768,2048]{1,0:T(8,128)(2,1)} %bitcast.10, s32[1024]{0:T(1024)S(1)} %pad_clamp_fusion.3), kind=kCustom, calls=%fused_computation.2.clone | custom fusion | bytes 4196352 | tf_op jit(solution)/shard_map/jit(_take)/gather | solution.py:26
  186.6 7.5 %gather_fusion.2 = bf16[512,2048]{1,0:T(8,128)(2,1)} fusion(bf16[768,2048]{1,0:T(8,128)(2,1)} %bitcast.10, s32[1024]{0:T(1024)S(1)} %pad_clamp_fusion.4), kind=kCustom, calls=%fused_computation.1.clone | custom fusion | bytes 4196352 | tf_op jit(solution)/shard_map/jit(_take)/gather | solution.py:26
  194.1 7.8 %gather_fusion.1 = bf16[512,2048]{1,0:T(8,128)(2,1)} fusion(bf16[768,2048]{1,0:T(8,128)(2,1)} %bitcast.10, s32[1024]{0:T(1024)S(1)} %pad_clamp_fusion.5), kind=kCustom, calls=%fused_computation.clone | custom fusion | bytes 4196352 | tf_op jit(solution)/shard_map/jit(_take)/gather | solution.py:26
  202.0 9.0 %multiply_add_fusion = f32[512,2048]{1,0:T(8,128)} fusion(bf16[512,2048]{1,0:T(8,128)(2,1)} %gather_fusion.6, bf16[512,2048]{1,0:T(8,128)(2,1)} %gather_fusion.5, bf16[512,2048]{1,0:T(8,128)(2,1)} %gather_fusion.4, bf16[512,2048]{1,0:T(8,128)(2,1)} %gather_fusion.3, bf16[512,2048]{1,0:T(8,128)(2,1)} %gather_fusion.2, bf16[512,2048]{1,0:T(8,128)(2,1)} %gather_fusion.1, ...), kind=kLoop, calls=%fused_computation.16 | loop fusion | flops 24117248 | bytes 16792576 | tf_op jit(solution)/shard_map/add | solution.py:27
  211.1 0.9 copy-done.3
  212.0 2.5 convolution_bitcast_fusion.1
  214.5 0.8 fusion.15
  215.3 0.1 copy.46
  215.4 0.2 reshape.338
  215.6 11.3 %all_to_all.29 = bf16[8,2,2048]{2,1,0:T(2,128)(2,1)S(1)} all-to-all(bf16[8,2,2048]{2,1,0:T(2,128)(2,1)S(1)} %reshape.338), channel_id=1, replica_groups=mesh['ep'=4,'tp'=8] {'tp'}, dimensions={0} | all-to-all | bytes 131072 | tf_op jit(solution)/shard_map/all_to_all | solution.py:64
  226.9 0.1 reshape.339
  227.0 0.1 copy.45
  227.1 0.1 all_to_all.25
  227.3 34.9 %reduce-scatter.2.cloned.1.call-done = f32[64,2048]{1,0:T(8,128)} async-done(((f32[512,2048]{1,0:T(8,128)}), f32[64,2048]{1,0:T(8,128)}) %reduce-scatter.2.cloned.1.call-update) | async-done | bytes 524304 | tf_op jit(solution)/shard_map/reduce_scatter | solution.py:93
  262.1 2.9 %fusion.6 = bf16[64,2048]{1,0:T(8,128)(2,1)} fusion(f32[64,2048]{1,0:T(8,128)} %reduce-scatter.2.cloned.1.call-done, bf16[512,64]{0,1:T(8,128)(2,1)S(1)} %all_to_all.25, bf16[512,2048]{1,0:T(8,128)(2,1)} %param.23), kind=kOutput, calls=%fused_computation.20 | convolution fusion | flops 134479872 | bytes 2949120 | tf_op jit(solution)/shard_map/dot_general | solution.py:65
  (50 shorter events, 0.4 us)
Async XLA Ops:
  6.5 100.9 %copy-start = (bf16[1,512,2048]{2,1,0:T(8,128)(2,1)S(1)}, bf16[1,512,2048]{2,1,0:T(8,128)(2,1)}, u32[]{:S(2)}) copy-start(bf16[1,512,2048]{2,1,0:T(8,128)(2,1)} %param.20) | copy-start | bytes 6291460
  6.5 35.8 %all-gather.2.cloned.1.call-start = ((), (), s32[]{:S(2)}) async-start(), calls=%async_computation.4 | async-start | bytes 2359296 | tf_op jit(solution)/shard_map/all_gather | solution.py:47
  42.3 2.2 copy-start.2
  42.3 2.9 %copy-start.5 = (f32[2048]{0:T(1024)S(1)}, f32[2048]{0:T(1024)}, u32[]{:S(2)}) copy-start(f32[2048]{0:T(1024)} %param.15) | copy-start | bytes 24580
  42.3 2.9 %copy-start.6 = (f32[2048]{0:T(1024)S(1)}, f32[2048]{0:T(1024)}, u32[]{:S(2)}) copy-start(f32[2048]{0:T(1024)} %param.14) | copy-start | bytes 24580
  60.3 5.3 %copy-start.4 = (f32[512,6]{0,1:T(8,128)S(1)}, f32[512,6]{0,1:T(8,128)}, u32[]{:S(2)}) copy-start(f32[512,6]{0,1:T(8,128)} %param.17) | copy-start | bytes 36868
  60.3 41.6 %all-to-all-start = ((bf16[4,8,24,2048]{3,2,1,0:T(8,128)(2,1)}), bf16[4,8,24,2048]{3,2,1,0:T(8,128)(2,1)}, u32[]{:S(2)}, u32[]{:S(2)}) async-start(bf16[4,8,24,2048]{3,2,1,0:T(8,128)(2,1)} %broadcast_select_fusion), calls=%async_computation | async-start | bytes 6291456 | tf_op jit(solution)/shard_map/all_to_all | solution.py:86
  115.6 40.6 %all-to-all-start.1 = ((bf16[4,8,24,2048]{3,2,1,0:T(8,128)(2,1)}), bf16[4,8,24,2048]{3,2,1,0:T(8,128)(2,1)}, u32[]{:S(2)}, u32[]{:S(2)}) async-start(bf16[4,8,24,2048]{3,2,1,0:T(8,128)(2,1)} %bitcast.78), calls=%async_computation.1 | async-start | bytes 6291456 | tf_op jit(solution)/shard_map/all_to_all | solution.py:88
  120.3 141.9 %reduce-scatter.2.cloned.1.call-start = ((), (), s32[]{:S(2)}) async-start(), calls=%async_computation.5 | async-start | bytes 4718592 | tf_op jit(solution)/shard_map/reduce_scatter | solution.py:93
  211.0 0.9 copy-start.3
  212.0 2.5 copy-start.1
  212.0 2.5 copy-start.7
Sparse Core Ops, SparseCore 0:
  8.9 33.3 all-gather.1
  211.2 50.8 reduce-scatter.1
where the time goes:
time: 273 us; the launch traced here: 272 us
  waiting for transfers between devices  120 us (44%)
  local copies, waits for them, and re-layouts  71.2 us (26%)
  other arithmetic  25.8 us (9%)
  matrix products  19.9 us (7%)
  between operations  13.8 us (5%)
  blocking collectives  11.3 us (4%)
  starting transfers between devices  9.63 us (4%)
    gather x6, local copies, waits for them, and re-layouts, weighted_sum(): jnp.take(source_rows, slot_index[:, column], axis=0, mode='fill', fill_va...  45.7 us
    all_to_all x1, waiting for transfers between devices, on_device(): lax.all_to_all(result.reshape(incoming.shape), 'ep', split_axis=0, concat...  35.7 us
    all_to_all x1, waiting for transfers between devices, on_device(): lax.all_to_all(outgoing, 'ep', split_axis=0, concat_axis=0, tiled=True)  35.2 us
    reduce_scatter x1, waiting for transfers between devices, on_device(): lax.psum_scatter(weighted_sum(back_rows, pair_slot, weights, top_count),...  34.9 us
    all_gather x1, waiting for transfers between devices, on_device(): whole = lax.all_gather(tokens, 'tp', axis=1, tiled=True)  13.8 us
    scatter x1, local copies, waits for them, and re-layouts, on_device(): source_row = jnp.full((slot_total + 1,), tok_count, jnp.int32).at[dest.re...  11.8 us
    all_to_all x1, blocking collectives, on_device(): lax.all_to_all(shared_hidden, 'tp', split_axis=1, concat_axis=0, tiled=True)  11.3 us
    add x1, other arithmetic, weighted_sum(): total + pair_weight[:, column:column + 1] * picked.astype(jnp.float32)  9.05 us
  transfers between devices with their start and end apart: 4, of which 4 were waited for; matrix products, arithmetic and copies ran while one was open for 10% of the time, Pallas kernels for 0%

commit v1 on v0

--- a/solution.py
+++ b/solution.py
@@ -44,7 +44,7 @@
     ep_count = lax.axis_size("ep")
     tp_count = lax.axis_size("tp")
     tp_index = lax.axis_index("tp")
-    whole = lax.all_gather(tokens, "tp", axis=1, tiled=True)
+    whole = jnp.concatenate(lax.all_gather(tokens, "tp"), axis=1)
     tok_count = whole.shape[0]
     width = whole.shape[1]
     top_count = expert_ids.shape[1]

time: 273 us -> 272 us (level)
  no operation moved by 1% of the time
where the time goes in v1:
time: 272 us; the launch traced here: 271 us
  waiting for transfers between devices  119 us (44%)
  local copies, waits for them, and re-layouts  71.8 us (26%)
  other arithmetic  27.4 us (10%)
  matrix products  19.9 us (7%)
  between operations  13.8 us (5%)
  blocking collectives  9.86 us (4%)
  starting transfers between devices  9.63 us (4%)
    gather x6, local copies, waits for them, and re-layouts, weighted_sum(): jnp.take(source_rows, slot_index[:, column], axis=0, mode='fill', fill_va...  45.7 us
    all_to_all x1, waiting for transfers between devices, on_device(): lax.all_to_all(result.reshape(incoming.shape), 'ep', split_axis=0, concat...  35.7 us
    all_to_all x1, waiting for transfers between devices, on_device(): lax.all_to_all(outgoing, 'ep', split_axis=0, concat_axis=0, tiled=True)  35.2 us
    reduce_scatter x1, waiting for transfers between devices, on_device(): lax.psum_scatter(weighted_sum(back_rows, pair_slot, weights, top_count),...  34.9 us
    all_gather x1, waiting for transfers between devices, on_device(): whole = jnp.concatenate(lax.all_gather(tokens, 'tp'), axis=1)  12.3 us
    scatter x1, local copies, waits for them, and re-layouts, on_device(): source_row = jnp.full((slot_total + 1,), tok_count, jnp.int32).at[dest.re...  11.8 us
    all_to_all x1, blocking collectives, on_device(): lax.all_to_all(shared_hidden, 'tp', split_axis=1, concat_axis=0, tiled=True)  9.86 us
    add x1, other arithmetic, weighted_sum(): total + pair_weight[:, column:column + 1] * picked.astype(jnp.float32)  9.05 us
  transfers between devices with their start and end apart: 4, of which 4 were waited for; matrix products, arithmetic and copies ran while one was open for 10% of the time, Pallas kernels for 0%

profile of v1, /device:TPU:0, one launch (start us, length us, event | category | flops | bytes accessed | tf_op | source)
XLA Modules:
  0.0 271.2 jit_solution(8193581339956051146)
XLA Ops:
  6.5 0.7 all-gather.3.cloned.1.call-update
  7.3 0.9 copy.50
  8.1 0.2 eq.48
  8.3 0.2 reshape.251
  8.5 0.2 eq.52
  8.8 6.9 %reduce-window.6 = s32[8,32,3,128]{3,1,2,0:T(8,128)S(1)} reduce-window(s32[8,32,3,128]{3,1,2,0:T(8,128)S(1)} %fusion.14, s32[]{:T(128)} %constant.82.clone.1), window={size=1x1x1x128 pad=0_0x0_0x0_0x127_0}, to_apply=%region_1.0 | reduce-window | flops 12484608 | bytes 786436 | tf_op jit(solution)/shard_map/reduce-window
  15.8 0.2 slice.78
  15.9 0.2 copy.56
  16.3 0.2 fusion.13
  16.5 0.1 compare_select_fusion
  16.6 11.8 %scatter_custom_fusion = s32[769]{0:T(1024)S(1)} fusion(s32[3072]{0:T(1024)S(1)} %bitcast.91, s32[3072]{0:T(1024)S(1)} %reshape.317, s32[]{:T(128)} %constant.81.clone.1), kind=kCustom, calls=%fused_computation.89 | custom fusion | bytes 3080 | tf_op jit(solution)/shard_map/scatter | solution.py:81
  28.4 0.1 slice.51
  28.5 12.3 %all-gather.3.cloned.1.call-done = bf16[4096,256]{1,0:T(8,128)(2,1)} async-done(((bf16[512,256]{1,0:T(8,128)(2,1)}), bf16[4096,256]{1,0:T(8,128)(2,1)}) %all-gather.3.cloned.1.call-update) | async-done | bytes 2097168 | tf_op jit(solution)/shard_map/all_gather | solution.py:47
  40.8 2.2 convert_reduce_fusion
  43.1 2.3 multiply_reduce_fusion
  45.4 0.6 copy.67
  46.0 0.1 copy-done.4
  46.1 2.1 add_convert_fusion
  48.2 9.0 %gather_fusion = bf16[768,2048]{1,0:T(8,128)(2,1)} fusion(bf16[512,2048]{1,0:T(8,128)(2,1)} %add_convert_fusion, s32[1024]{0:T(1024)S(1)} %pad_clamp_fusion.6), kind=kCustom, calls=%fused_computation.6 | custom fusion | bytes 6294528 | tf_op jit(solution)/shard_map/jit(_take)/gather | solution.py:83
  57.2 3.9 %broadcast_select_fusion = bf16[4,8,24,2048]{3,2,1,0:T(8,128)(2,1)} fusion(bf16[4,8,24,2048]{3,2,1,0:T(8,128)(2,1)} %bitcast.85, pred[4,8,24]{2,1,0:T(8,128)(4,1)S(1)} %compare_and_fusion), kind=kLoop, calls=%fused_computation.12 | loop fusion | flops 1572864 | bytes 6292224 | tf_op jit(solution)/shard_map/jit(_take)/select_n | solution.py:83
  61.1 4.9 %all-to-all-start = ((bf16[4,8,24,2048]{3,2,1,0:T(8,128)(2,1)}), bf16[4,8,24,2048]{3,2,1,0:T(8,128)(2,1)}, u32[]{:S(2)}, u32[]{:S(2)}) async-start(bf16[4,8,24,2048]{3,2,1,0:T(8,128)(2,1)} %broadcast_select_fusion), calls=%async_computation | async-start | bytes 6291456 | tf_op jit(solution)/shard_map/all_to_all | solution.py:86
  66.1 0.1 add.204
  66.1 0.2 sub.45
  66.4 0.3 fusion.20
  66.6 0.8 slice_reduce_fusion.5
  67.5 35.2 %all-to-all-done = bf16[4,8,24,2048]{3,2,1,0:T(8,128)(2,1)} async-done(((bf16[4,8,24,2048]{3,2,1,0:T(8,128)(2,1)}), bf16[4,8,24,2048]{3,2,1,0:T(8,128)(2,1)}, u32[]{:S(2)}, u32[]{:S(2)}) %all-to-all-start) | async-done | bytes 3145760 | tf_op jit(solution)/shard_map/all_to_all | solution.py:86
  102.7 5.6 %fusion.4 = f32[768,512]{1,0:T(8,128)} fusion(bf16[768,2048]{1,0:T(8,128)(2,1)} %bitcast.7, bf16[1,2048,512]{2,1,0:T(8,128)(2,1)} %param.18), kind=kOutput, calls=%fused_computation.18 | convolution fusion | flops 1610612736 | bytes 6815744 | tf_op jit(solution)/shard_map/dot_general | solution.py:17
  108.2 8.2 %convolution_convert_fusion = bf16[768,2048]{1,0:T(8,128)(2,1)} fusion(bf16[1,512,2048]{2,1,0:T(8,128)(2,1)S(1)} %copy-done, f32[768,512]{1,0:T(8,128)} %fusion.4, bf16[768,2048]{1,0:T(8,128)(2,1)} %bitcast.7, bf16[1,2048,512]{2,1,0:T(8,128)(2,1)} %param.19), kind=kOutput, calls=%fused_computation.11 | convolution fusion | flops 3225157632 | bytes 12058624 | tf_op jit(solution)/shard_map/dot_general | solution.py:20
  116.4 4.6 %all-to-all-start.1 = ((bf16[4,8,24,2048]{3,2,1,0:T(8,128)(2,1)}), bf16[4,8,24,2048]{3,2,1,0:T(8,128)(2,1)}, u32[]{:S(2)}, u32[]{:S(2)}) async-start(bf16[4,8,24,2048]{3,2,1,0:T(8,128)(2,1)} %bitcast.87), calls=%async_computation.1 | async-start | bytes 6291456 | tf_op jit(solution)/shard_map/all_to_all | solution.py:88
  121.3 35.7 %all-to-all-done.1 = bf16[4,8,24,2048]{3,2,1,0:T(8,128)(2,1)} async-done(((bf16[4,8,24,2048]{3,2,1,0:T(8,128)(2,1)}), bf16[4,8,24,2048]{3,2,1,0:T(8,128)(2,1)}, u32[]{:S(2)}, u32[]{:S(2)}) %all-to-all-start.1) | async-done | bytes 3145760 | tf_op jit(solution)/shard_map/all_to_all | solution.py:88
  157.0 7.8 %gather_fusion.6 = bf16[512,2048]{1,0:T(8,128)(2,1)} fusion(bf16[768,2048]{1,0:T(8,128)(2,1)} %bitcast.12, s32[1024]{0:T(1024)S(1)} %pad_clamp_fusion), kind=kCustom, calls=%fused_computation.5.clone | custom fusion | bytes 4196352 | tf_op jit(solution)/shard_map/jit(_take)/gather | solution.py:26
  164.8 7.5 %gather_fusion.5 = bf16[512,2048]{1,0:T(8,128)(2,1)} fusion(bf16[768,2048]{1,0:T(8,128)(2,1)} %bitcast.12, s32[1024]{0:T(1024)S(1)} %pad_clamp_fusion.1), kind=kCustom, calls=%fused_computation.4.clone | custom fusion | bytes 4196352 | tf_op jit(solution)/shard_map/jit(_take)/gather | solution.py:26
  172.3 7.5 %gather_fusion.4 = bf16[512,2048]{1,0:T(8,128)(2,1)} fusion(bf16[768,2048]{1,0:T(8,128)(2,1)} %bitcast.12, s32[1024]{0:T(1024)S(1)} %pad_clamp_fusion.2), kind=kCustom, calls=%fused_computation.3.clone | custom fusion | bytes 4196352 | tf_op jit(solution)/shard_map/jit(_take)/gather | solution.py:26
  179.9 7.5 %gather_fusion.3 = bf16[512,2048]{1,0:T(8,128)(2,1)} fusion(bf16[768,2048]{1,0:T(8,128)(2,1)} %bitcast.12, s32[1024]{0:T(1024)S(1)} %pad_clamp_fusion.3), kind=kCustom, calls=%fused_computation.2.clone | custom fusion | bytes 4196352 | tf_op jit(solution)/shard_map/jit(_take)/gather | solution.py:26
  187.4 7.5 %gather_fusion.2 = bf16[512,2048]{1,0:T(8,128)(2,1)} fusion(bf16[768,2048]{1,0:T(8,128)(2,1)} %bitcast.12, s32[1024]{0:T(1024)S(1)} %pad_clamp_fusion.4), kind=kCustom, calls=%fused_computation.1.clone | custom fusion | bytes 4196352 | tf_op jit(solution)/shard_map/jit(_take)/gather | solution.py:26
  194.9 7.8 %gather_fusion.1 = bf16[512,2048]{1,0:T(8,128)(2,1)} fusion(bf16[768,2048]{1,0:T(8,128)(2,1)} %bitcast.12, s32[1024]{0:T(1024)S(1)} %pad_clamp_fusion.5), kind=kCustom, calls=%fused_computation.clone | custom fusion | bytes 4196352 | tf_op jit(solution)/shard_map/jit(_take)/gather | solution.py:26
  202.8 9.0 %multiply_add_fusion = f32[512,2048]{1,0:T(8,128)} fusion(bf16[512,2048]{1,0:T(8,128)(2,1)} %gather_fusion.6, bf16[512,2048]{1,0:T(8,128)(2,1)} %gather_fusion.5, bf16[512,2048]{1,0:T(8,128)(2,1)} %gather_fusion.4, bf16[512,2048]{1,0:T(8,128)(2,1)} %gather_fusion.3, bf16[512,2048]{1,0:T(8,128)(2,1)} %gather_fusion.2, bf16[512,2048]{1,0:T(8,128)(2,1)} %gather_fusion.1, ...), kind=kLoop, calls=%fused_computation.8 | loop fusion | flops 24117248 | bytes 16792576 | tf_op jit(solution)/shard_map/add | solution.py:27
  211.8 0.9 copy-done.2
  212.8 2.5 convolution_bitcast_fusion.1
  215.3 0.8 fusion.9
  216.1 0.1 copy.63
  216.2 0.2 reshape.352
  216.4 9.9 %all_to_all.29 = bf16[8,2,2048]{2,1,0:T(2,128)(2,1)S(1)} all-to-all(bf16[8,2,2048]{2,1,0:T(2,128)(2,1)S(1)} %reshape.352), channel_id=1, replica_groups=mesh['ep'=4,'tp'=8] {'tp'}, dimensions={0} | all-to-all | bytes 131072 | tf_op jit(solution)/shard_map/all_to_all | solution.py:64
  226.2 0.1 reshape.353
  226.4 0.1 copy.62
  226.5 0.1 all_to_all.25
  226.6 34.9 %reduce-scatter.2.cloned.1.call-done = f32[64,2048]{1,0:T(8,128)} async-done(((f32[512,2048]{1,0:T(8,128)}), f32[64,2048]{1,0:T(8,128)}) %reduce-scatter.2.cloned.1.call-update) | async-done | bytes 524304 | tf_op jit(solution)/shard_map/reduce_scatter | solution.py:93
  261.5 2.9 %fusion = bf16[64,2048]{1,0:T(8,128)(2,1)} fusion(f32[64,2048]{1,0:T(8,128)} %reduce-scatter.2.cloned.1.call-done, bf16[512,64]{0,1:T(8,128)(2,1)S(1)} %all_to_all.25, bf16[512,2048]{1,0:T(8,128)(2,1)} %param.23), kind=kOutput, calls=%fused_computation.14 | convolution fusion | flops 134479872 | bytes 2949120 | tf_op jit(solution)/shard_map/dot_general | solution.py:65
  (51 shorter events, 0.5 us)
Async XLA Ops:
  6.5 101.7 %copy-start = (bf16[1,512,2048]{2,1,0:T(8,128)(2,1)S(1)}, bf16[1,512,2048]{2,1,0:T(8,128)(2,1)}, u32[]{:S(2)}) copy-start(bf16[1,512,2048]{2,1,0:T(8,128)(2,1)} %param.20) | copy-start | bytes 6291460
  6.5 34.3 %all-gather.3.cloned.1.call-start = ((), (), s32[]{:S(2)}) async-start(), calls=%async_computation.5 | async-start | bytes 2359296 | tf_op jit(solution)/shard_map/all_gather | solution.py:47
  45.4 0.7 copy-start.4
  45.4 0.7 copy-start.5
  61.1 5.0 %copy-start.3 = (f32[512,6]{0,1:T(8,128)S(1)}, f32[512,6]{0,1:T(8,128)}, u32[]{:S(2)}) copy-start(f32[512,6]{0,1:T(8,128)} %param.17) | copy-start | bytes 36868
  61.1 41.6 %all-to-all-start = ((bf16[4,8,24,2048]{3,2,1,0:T(8,128)(2,1)}), bf16[4,8,24,2048]{3,2,1,0:T(8,128)(2,1)}, u32[]{:S(2)}, u32[]{:S(2)}) async-start(bf16[4,8,24,2048]{3,2,1,0:T(8,128)(2,1)} %broadcast_select_fusion), calls=%async_computation | async-start | bytes 6291456 | tf_op jit(solution)/shard_map/all_to_all | solution.py:86
  116.4 40.6 %all-to-all-start.1 = ((bf16[4,8,24,2048]{3,2,1,0:T(8,128)(2,1)}), bf16[4,8,24,2048]{3,2,1,0:T(8,128)(2,1)}, u32[]{:S(2)}, u32[]{:S(2)}) async-start(bf16[4,8,24,2048]{3,2,1,0:T(8,128)(2,1)} %bitcast.87), calls=%async_computation.1 | async-start | bytes 6291456 | tf_op jit(solution)/shard_map/all_to_all | solution.py:88
  121.1 140.4 %reduce-scatter.2.cloned.1.call-start = ((), (), s32[]{:S(2)}) async-start(), calls=%async_computation.4 | async-start | bytes 4718592 | tf_op jit(solution)/shard_map/reduce_scatter | solution.py:93
  211.8 0.9 copy-start.2
  212.8 2.5 copy-start.1
  212.8 2.5 copy-start.6
Sparse Core Ops, SparseCore 0:
  8.9 31.8 all-gather.2
  212.0 49.4 reduce-scatter.1
